TPU v7x, 32 devices: a whole 2x2x4 slice. The times are simulated.
32 devices in a mesh: st: 8 (over z, y), tp: 4 (over x, core).
Axes of the slice: x: 2, y: 2, z: 4, core: 2. Of those that a mesh axis runs over, the one named last changes fastest.
Arguments:
- queries: bfloat16 [8192, 1024], P('st', 'tp'), may hold values from -540 to 540
- gate_pre: bfloat16 [8192, 1024], P('st', 'tp'), may hold values from -6 to 6
- cotangent: bfloat16 [8192, 1024], P('st', 'tp'), may hold values from -6 to 6
- store: bfloat16 [10240, 2048], P('st'), may hold values from -6 to 6
- store_gain: float32 [2048], replicated, may hold values from 0.1 to 1.9
- w_key: bfloat16 [2048, 1024], P(None, 'tp'), may hold values from -0.125 to 0.125
- w_value: bfloat16 [2048, 1024], P(None, 'tp'), may hold values from -0.125 to 0.125
- owners: int32 [64, 4], P('st'), may hold values from 0 to 7, all different within a row; in each aligned block of 8 rows (0 to 7, 8 to 15, ...) at most 8 rows name the same one
- slots: int32 [64, 4], P('st'), may hold values from 0 to 19
Outputs:
- grad_queries: float32 [8192, 1024], P('st', 'tp')
- grad_store: float32 [10240, 2048], P(('st', 'tp'))
- grad_w_value: float32 [2048, 1024], P('st', 'tp')
Inputs may be any that keep to these rules, and one draw needn't show every extreme that they name: Each block names 4 different owners. Among the blocks of one device no owner is named twice.
All inputs are finite; a program needn't handle non-finite values.
Results may differ from a plain program's by a relative error of at most 0.014.
Values may be sent and summed in bfloat16 or wider, within the bound.
A program may use at most 192 MiB of HBM per device.

v0:
```python
import functools

import jax
import jax.numpy as jnp
from jax import lax
from jax.experimental import pallas as pl
from jax.experimental.pallas import tpu as pltpu
from jax.sharding import PartitionSpec as P

HD = 128
PLEN = 64


EPS = 1e-06


def row_scale(store_rows):
    return lax.rsqrt(jnp.mean(store_rows * store_rows, axis=-1, keepdims=True) + EPS)


def contract(left, right):
    return lax.dot_general(
        left, right, (((1,), (1,)), ((), ())), preferred_element_type=jnp.float32
    )


def passage_plan(queries, gate_pre, cotangent, store, store_gain, w_key, w_value, owners, slots):
    st_size = lax.axis_size("st")
    tp_size = lax.axis_size("tp")
    blocks, per_block = owners.shape
    tok_rows, local_width = queries.shape
    head_dim = HD
    local_heads = local_width // head_dim
    block_len = tok_rows // blocks
    passage_len = PLEN
    rows_dev = store.shape[0]
    passages = rows_dev // passage_len
    slot_count = blocks * per_block
    slot_cap = (2 * slot_count + st_size - 1) // st_size
    store_rows = store.astype(jnp.float32)
    row_inverse = row_scale(store_rows)
    normed = (store_rows * row_inverse * store_gain).astype(jnp.bfloat16)
    key_table = jnp.dot(normed, w_key, preferred_element_type=jnp.float32).astype(jnp.bfloat16)
    value_table = jnp.dot(normed, w_value, preferred_element_type=jnp.float32).astype(jnp.bfloat16)
    key_table = key_table.reshape(passages, passage_len, local_width)
    value_table = value_table.reshape(passages, passage_len, local_width)
    owner_flat = owners.reshape(slot_count)
    slot_flat = slots.reshape(slot_count)
    slot_order = jnp.arange(slot_count, dtype=jnp.int32)
    earlier_same = (owner_flat[:, None] == owner_flat[None, :]) & (
        slot_order[None, :] < slot_order[:, None]
    )
    slot_rank = jnp.sum(earlier_same.astype(jnp.int32), axis=1)
    position = owner_flat * slot_cap + slot_rank
    places = jnp.arange(st_size * slot_cap, dtype=jnp.int32)
    slot_hits = position[:, None] == places[None, :]
    requests = jnp.sum(jnp.where(slot_hits, slot_flat[:, None], 0), axis=0)
    requests = requests.reshape(st_size, slot_cap)
    asked_ids = lax.all_to_all(requests, "st", split_axis=0, concat_axis=0, tiled=True)
    asked_flat = asked_ids.reshape(-1)
    shape_out = asked_ids.shape + (passage_len, local_width)
    picked_keys = jnp.take(key_table, asked_flat, axis=0).reshape(shape_out)
    picked_values = jnp.take(value_table, asked_flat, axis=0).reshape(shape_out)
    sent_keys = lax.all_to_all(picked_keys, "st", split_axis=0, concat_axis=0, tiled=True)
    sent_values = lax.all_to_all(picked_values, "st", split_axis=0, concat_axis=0, tiled=True)
    got_keys, got_values, asked_ids = (sent_keys, sent_values, asked_ids)
    span = per_block * passage_len
    mine_keys = jnp.take(
        got_keys.reshape(st_size * slot_cap, passage_len, local_width), position, axis=0
    )
    mine_values = jnp.take(
        got_values.reshape(st_size * slot_cap, passage_len, local_width), position, axis=0
    )
    mine_keys = mine_keys.reshape(blocks, span, local_heads, head_dim)
    mine_values = mine_values.reshape(blocks, span, local_heads, head_dim)
    score_scale = head_dim ** (-0.5)
    query_blocks = queries.reshape(blocks, block_len, local_heads, head_dim)
    gate_open = jax.nn.sigmoid(gate_pre.astype(jnp.float32))
    grad_in = (gate_open * cotangent.astype(jnp.float32)).astype(jnp.bfloat16)
    grad_in = grad_in.reshape(blocks, block_len, local_heads, head_dim)
    scores = (
        jnp.einsum("bqhd,bkhd->bhqk", query_blocks, mine_keys, preferred_element_type=jnp.float32)
        * score_scale
    )
    shifted = scores - jnp.max(scores, axis=-1, keepdims=True)
    weights = jnp.exp(shifted)
    weights = weights / jnp.sum(weights, axis=-1, keepdims=True)
    weights_half = weights.astype(jnp.bfloat16)
    attended = jnp.einsum(
        "bhqk,bkhd->bqhd", weights_half, mine_values, preferred_element_type=jnp.float32
    )
    row_delta = jnp.sum(grad_in.astype(jnp.float32) * attended, axis=-1)
    grad_weights = jnp.einsum(
        "bqhd,bkhd->bhqk", grad_in, mine_values, preferred_element_type=jnp.float32
    )
    grad_scores = weights * (grad_weights - jnp.transpose(row_delta, (0, 2, 1))[..., None])
    grad_half = grad_scores.astype(jnp.bfloat16)
    grad_queries = (
        jnp.einsum("bhqk,bkhd->bqhd", grad_half, mine_keys, preferred_element_type=jnp.float32)
        * score_scale
    )
    grad_queries = grad_queries.reshape(tok_rows, local_width)
    grad_keys = (
        jnp.einsum("bhqk,bqhd->bkhd", grad_half, query_blocks, preferred_element_type=jnp.float32)
        * score_scale
    )
    grad_values = jnp.einsum(
        "bhqk,bqhd->bkhd", weights_half, grad_in, preferred_element_type=jnp.float32
    )
    grad_keys = grad_keys.reshape(slot_count, passage_len, local_width)
    grad_values = grad_values.reshape(slot_count, passage_len, local_width)
    empty_slots = jnp.zeros((st_size * slot_cap, passage_len, local_width), jnp.bfloat16)
    outgoing_keys = empty_slots.at[position].set(grad_keys.astype(jnp.bfloat16))
    outgoing_values = empty_slots.at[position].set(grad_values.astype(jnp.bfloat16))
    back_keys, back_values = (
        lax.all_to_all(outgoing_keys, "st", split_axis=0, concat_axis=0, tiled=True),
        lax.all_to_all(outgoing_values, "st", split_axis=0, concat_axis=0, tiled=True),
    )
    asked_flat = asked_ids.reshape(-1)
    owner_pick = (asked_flat[None, :] == jnp.arange(passages, dtype=jnp.int32)[:, None]).astype(
        jnp.bfloat16
    )
    passage_keys = jnp.dot(
        owner_pick,
        back_keys.reshape(st_size * slot_cap, passage_len * local_width),
        preferred_element_type=jnp.float32,
    )
    passage_values = jnp.dot(
        owner_pick,
        back_values.reshape(st_size * slot_cap, passage_len * local_width),
        preferred_element_type=jnp.float32,
    )
    passage_keys = passage_keys.astype(jnp.bfloat16).reshape(rows_dev, local_width)
    passage_values = passage_values.astype(jnp.bfloat16).reshape(rows_dev, local_width)
    weight_terms = lax.dot_general(
        normed, passage_values, (((0,), (0,)), ((), ())), preferred_element_type=jnp.float32
    )
    grad_w_value = lax.psum_scatter(weight_terms, "st", scatter_dimension=0, tiled=True)
    quarter = rows_dev // tp_size
    whole_key, whole_value = (
        lax.all_gather(w_key, "tp", axis=1, tiled=True),
        lax.all_gather(w_value, "tp", axis=1, tiled=True),
    )
    own_keys, own_values = (
        lax.all_to_all(passage_keys, "tp", split_axis=0, concat_axis=1, tiled=True),
        lax.all_to_all(passage_values, "tp", split_axis=0, concat_axis=1, tiled=True),
    )
    grad_normed = contract(own_keys, whole_key) + contract(own_values, whole_value)
    first_row = lax.axis_index("tp") * quarter
    own_rows = lax.dynamic_slice_in_dim(store_rows, first_row, quarter, 0)
    own_inverse = lax.dynamic_slice_in_dim(row_inverse, first_row, quarter, 0)
    unit_rows = own_rows * own_inverse
    grad_unit = grad_normed * store_gain
    grad_store = own_inverse * (
        grad_unit - unit_rows * jnp.mean(grad_unit * unit_rows, axis=-1, keepdims=True)
    )
    return (grad_queries, grad_store, grad_w_value)


FAR = -1e30
MESH = pl.DeviceIdType.MESH


def place_of(index, n):
    odd = index % 2
    return (1 - odd) * (index // 2) + odd * (n - 1 - index // 2)


def index_at(place, n):
    place = (place + 2 * n) % n
    back = place // (n // 2)
    return (1 - back) * (2 * place) + back * (2 * (n - 1 - place) + 1)


def greet(others):
    barrier = pltpu.get_barrier_semaphore()
    for axis, other in others:
        pl.semaphore_signal(barrier, inc=1, device_id={axis: other}, device_id_type=MESH)
    pl.semaphore_wait(barrier, len(others))


def gather_kernel(n, q_ref, g_ref, i_ref, q_all, g_all, i_all, send_sem, recv_sem, own_sem):
    me = lax.axis_index("st")
    place = place_of(me, n)
    right, left = index_at(place + 1, n), index_at(place - 1, n)
    half_rows = q_ref.shape[0] // 2
    pairs = ((q_ref, q_all), (g_ref, g_all), (i_ref, i_all))
    greet((("st", left), ("st", right)))
    own = []
    for number, (src, dst) in enumerate(pairs):
        copy = pltpu.make_async_copy(src, dst.at[me], own_sem.at[number])
        copy.start()
        own.append(copy)
    hops = n // 2
    parts = ((2, 0), (0, 0), (0, 1), (1, 0), (1, 1))

    def last_on(side, part):
        return parts[part][1] == side

    def piece(side, step, part):
        number, half = parts[part]
        src, dst = pairs[number]
        origin = index_at(place - step, n) if side == 0 else index_at(place + step, n)
        rows = pl.ds(0, i_ref.shape[0]) if number == 2 else pl.ds(half * half_rows, half_rows)
        return pltpu.make_async_remote_copy(
            src_ref=src.at[rows] if step == 0 else dst.at[origin, rows],
            dst_ref=dst.at[origin, rows],
            send_sem=send_sem.at[side, step, part],
            recv_sem=recv_sem.at[side, step, part],
            device_id={"st": right if side == 0 else left},
            device_id_type=MESH,
        )

    started = []
    for step in range(hops):
        for part in range(5):
            for side in range(2):
                if step < hops - 1 or last_on(side, part):
                    if step > 0:
                        piece(side, step - 1, part).wait_recv()
                    copy = piece(side, step, part)
                    copy.start()
                    started.append(copy)
    for part in range(5):
        for side in range(2):
            if not last_on(side, part):
                piece(side, hops - 2, part).wait_recv()
    for part in range(5):
        piece(parts[part][1], hops - 1, part).wait_recv()
    for copy in own:
        copy.wait()
    for copy in started:
        copy.wait_send()


def ring_gather(queries, grad_in, named, n):
    hops = n // 2
    vmem = pl.BlockSpec(memory_space=pltpu.VMEM)
    sources = (queries, grad_in, named)
    return pl.pallas_call(
        functools.partial(gather_kernel, n),
        out_shape=tuple(jax.ShapeDtypeStruct((n,) + x.shape, x.dtype) for x in sources),
        in_specs=[vmem] * 3,
        out_specs=(vmem,) * 3,
        scratch_shapes=[
            pltpu.SemaphoreType.DMA((2, hops, 5)),
            pltpu.SemaphoreType.DMA((2, hops, 5)),
            pltpu.SemaphoreType.DMA((3,)),
        ],
        cost_estimate=pl.CostEstimate(flops=10**10, bytes_accessed=10**7, transcendentals=0),
        compiler_params=pltpu.CompilerParams(collective_id=0, has_side_effects=True, vmem_limit_bytes=40 << 20),
        name="ring_gather",
    )(*sources)


def join_kernel(n, heads, x_ref, out_ref, got, mine, send_sem, recv_sem, own_sem):
    me = lax.axis_index("st")
    peers = [(me + away) % n for away in range(1, n)]
    greet([("st", peer) for peer in peers])

    def piece(phase, away):
        peer = (me + away) % n
        return pltpu.make_async_remote_copy(
            src_ref=x_ref.at[peer] if phase == 0 else mine,
            dst_ref=got.at[me] if phase == 0 else out_ref.at[me],
            send_sem=send_sem.at[phase, away],
            recv_sem=recv_sem.at[phase, away],
            device_id={"st": peer},
            device_id_type=MESH,
        )

    for away in range(1, n):
        piece(0, away).start()
    local = pltpu.make_async_copy(x_ref.at[me], got.at[me], own_sem.at[0])
    local.start()
    local.wait()
    for away in range(1, n):
        piece(0, away).wait()
    for head in range(heads):
        logs = [got[owner, :, 2 * head] for owner in range(n)]
        top = functools.reduce(jnp.maximum, logs)
        shares = [jnp.exp(one - top) for one in logs]
        total = sum(shares)
        mine[:, 2 * head] = top + jnp.log(total)
        mine[:, 2 * head + 1] = sum(share * got[owner, :, 2 * head + 1] for owner, share in enumerate(shares)) / total
    out_ref[me] = mine[...]
    for away in range(1, n):
        piece(1, away).start()
    for away in range(1, n):
        piece(1, away).wait()


def join_stats(stats, n):
    total, rows, width = stats.shape
    blocks = total // n
    vmem = pl.BlockSpec(memory_space=pltpu.VMEM)
    joined = pl.pallas_call(
        functools.partial(join_kernel, n, rows // 2),
        out_shape=jax.ShapeDtypeStruct((n, blocks, rows, width), jnp.float32),
        in_specs=[vmem],
        out_specs=vmem,
        scratch_shapes=[
            pltpu.VMEM((n, blocks, rows, width), jnp.float32),
            pltpu.VMEM((blocks, rows, width), jnp.float32),
            pltpu.SemaphoreType.DMA((2, n)),
            pltpu.SemaphoreType.DMA((2, n)),
            pltpu.SemaphoreType.DMA((1,)),
        ],
        cost_estimate=pl.CostEstimate(flops=10**9, bytes_accessed=10**6, transcendentals=0),
        compiler_params=pltpu.CompilerParams(collective_id=2, has_side_effects=True),
        name="join_stats",
    )(stats.reshape(n, blocks, rows, width))
    return joined.reshape(total, rows, width)


def scatter_kernel(n, tp, parts, x_ref, w_ref, k_ref, v_ref, out_ref, gw_ref, ok_ref, ov_ref, send_buf, recv_buf, send_sem, recv_sem, tp_send, tp_recv, own_sem):
    me = lax.axis_index("st")
    mine = lax.axis_index("tp")
    place = place_of(me, n)
    right, left = index_at(place + 1, n), index_at(place - 1, n)
    tokens = x_ref.shape[1]
    greet([("st", left), ("st", right)] + [("tp", (mine + away) % tp) for away in range(1, tp)])
    quarter, width = ok_ref.shape[0], k_ref.shape[1]
    columns = pl.ds(pl.multiple_of(mine * width, 128), width)

    def across(number, away):
        src, dst = ((k_ref, ok_ref), (v_ref, ov_ref))[number]
        peer = (mine + away) % tp
        return pltpu.make_async_remote_copy(
            src_ref=src.at[pl.ds(pl.multiple_of(peer * quarter, 16), quarter)],
            dst_ref=dst.at[:, columns],
            send_sem=tp_send.at[number, away],
            recv_sem=tp_recv.at[number, away],
            device_id={"tp": peer},
            device_id_type=MESH,
        )

    def kept(number):
        src, dst = ((k_ref, ok_ref), (v_ref, ov_ref))[number]
        return pltpu.make_async_copy(
            src.at[pl.ds(pl.multiple_of(mine * quarter, 16), quarter)], dst.at[:, columns], own_sem.at[number]
        )

    for number in range(2):
        kept(number).start()
        for away in range(1, tp):
            across(number, away).start()
    hops = n // 2

    def used(side, step, part):
        return step > 0 or parts[part][3] == side

    def piece(side, step, part):
        number, first, count, _ = parts[part]
        at = pl.ds(number * tokens + first, count)
        return pltpu.make_async_remote_copy(
            src_ref=send_buf.at[side, step, at],
            dst_ref=recv_buf.at[side, step, at],
            send_sem=send_sem.at[side, step, part],
            recv_sem=recv_sem.at[side, step, part],
            device_id={"st": right if side == 0 else left},
            device_id_type=MESH,
        )

    started = []
    for step in range(hops):
        for part, (number, first, count, _) in enumerate(parts):
            for side in range(2):
                if not used(side, step, part):
                    continue
                distance = hops - step
                dest = index_at(place + distance, n) if side == 0 else index_at(place - distance, n)
                at = pl.ds(number * tokens + first, count)
                total = (x_ref, w_ref)[number][dest, pl.ds(first, count)]
                if step > 0 and used(side, step - 1, part):
                    piece(side, step - 1, part).wait_recv()
                    total = (total.astype(jnp.float32) + recv_buf[side, step - 1, at].astype(jnp.float32)).astype(jnp.bfloat16)
                send_buf[side, step, at] = total
                copy = piece(side, step, part)
                copy.start()
                started.append(copy)
    for part, (number, first, count, _) in enumerate(parts):
        at = pl.ds(number * tokens + first, count)
        total = (x_ref, w_ref)[number][me, pl.ds(first, count)].astype(jnp.float32)
        for side in range(2):
            piece(side, hops - 1, part).wait_recv()
            total = total + recv_buf[side, hops - 1, at].astype(jnp.float32)
        (out_ref, gw_ref)[number][pl.ds(first, count)] = total
    for number in range(2):
        kept(number).wait()
        for away in range(1, tp):
            across(number, away).wait()
    for copy in started:
        copy.wait_send()


def ring_scatter(terms, weight_terms, keys, values, n, tp):
    rows, width = terms.shape[1:]
    rest = weight_terms.shape[1]
    hops = n // 2
    parts = ((0, 0, rows // 4, 0), (0, rows // 2, rows // 4, 1), (0, rows // 4, rows // 4, 0),
             (0, 3 * rows // 4, rows // 4, 1), (1, 0, rest // 2, 0), (1, rest // 2, rest // 2, 1))
    vmem = pl.BlockSpec(memory_space=pltpu.VMEM)
    own = jax.ShapeDtypeStruct((keys.shape[0] // tp, width * tp), jnp.bfloat16)
    return pl.pallas_call(
        functools.partial(scatter_kernel, n, tp, parts),
        out_shape=(
            jax.ShapeDtypeStruct((rows, width), jnp.float32),
            jax.ShapeDtypeStruct((rest, width), jnp.float32),
            own,
            own,
        ),
        in_specs=[vmem] * 4,
        out_specs=(vmem,) * 4,
        scratch_shapes=[
            pltpu.VMEM((2, hops, rows + rest, width), jnp.bfloat16),
            pltpu.VMEM((2, hops, rows + rest, width), jnp.bfloat16),
            pltpu.SemaphoreType.DMA((2, hops, len(parts))),
            pltpu.SemaphoreType.DMA((2, hops, len(parts))),
            pltpu.SemaphoreType.DMA((2, tp)),
            pltpu.SemaphoreType.DMA((2, tp)),
            pltpu.SemaphoreType.DMA((2,)),
        ],
        cost_estimate=pl.CostEstimate(flops=5 * 10**9, bytes_accessed=10**7, transcendentals=0),
        compiler_params=pltpu.CompilerParams(collective_id=1, has_side_effects=True, vmem_limit_bytes=50 << 20),
        name="ring_scatter",
    )(terms, weight_terms, keys, values)


NT = (((1,), (1,)), ((), ()))
TN = (((0,), (0,)), ((), ()))


def dot(left, right, dims=(((1,), (0,)), ((), ()))):
    return lax.dot_general(left, right, dims, preferred_element_type=jnp.float32)


def items_of(table, total, heads, turn):
    items = []
    for lane in range(2):
        block = table[total + 2 * turn + lane]
        picked = table[block]
        for head in range(heads):
            items.append((block, picked >= 0, jnp.maximum(picked, 0), head, pl.ds(head * HD, HD)))
    return items


def raw_products(items, q_ref, g_ref, k_ref, v_ref):
    scale = HD ** (-0.5)
    scores = [dot(k_ref[picked, :, cols], q_ref[block, :, cols], NT) * scale for block, _, picked, _, cols in items]
    grads = [dot(v_ref[picked, :, cols], g_ref[block, :, cols], NT) for block, _, picked, _, cols in items]
    return scores, grads


def stats_kernel(heads, table, q_ref, g_ref, k_ref, v_ref, out_ref):
    total, _, block_len = out_ref.shape

    @pl.loop(0, total)
    def _(block):
        for head in range(heads):
            out_ref[block, 2 * head] = jnp.full((block_len,), FAR, jnp.float32)
            out_ref[block, 2 * head + 1] = jnp.zeros((block_len,), jnp.float32)

    @pl.loop(0, (table[2 * total] + 1) // 2)
    def _(turn):
        items = items_of(table, total, heads, turn)
        scores, grads = raw_products(items, q_ref, g_ref, k_ref, v_ref)
        tops = [jnp.max(one, axis=0, keepdims=True) for one in scores]
        raised = [jnp.exp(one - top) for one, top in zip(scores, tops)]
        totals = [jnp.sum(one, axis=0, keepdims=True) for one in raised]
        means = [jnp.sum(one * two, axis=0, keepdims=True) / three for one, two, three in zip(raised, grads, totals)]
        logs = [top + jnp.log(one) for top, one in zip(tops, totals)]
        for number, (block, live, _, head, _) in enumerate(items):
            @pl.when(live)
            def _():
                out_ref[block, pl.ds(2 * head, 1)] = logs[number]
                out_ref[block, pl.ds(2 * head + 1, 1)] = means[number]


def grads_kernel(heads, table, q_ref, g_ref, k_ref, v_ref, s_ref, dq_ref, pk_ref, pv_ref, dk_acc, dv_acc):
    scale = HD ** (-0.5)
    total = dq_ref.shape[0]
    dk_acc[...] = jnp.zeros_like(dk_acc)
    dv_acc[...] = jnp.zeros_like(dv_acc)

    @pl.loop(table[2 * total], total)
    def _(at):
        dq_ref[table[total + at]] = jnp.zeros(dq_ref.shape[1:], jnp.bfloat16)

    @pl.loop(0, (table[2 * total] + 1) // 2)
    def _(turn):
        items = items_of(table, total, heads, turn)
        scores, grads = raw_products(items, q_ref, g_ref, k_ref, v_ref)
        weights, halves = [], []
        for (block, _, _, head, _), score, grad in zip(items, scores, grads):
            weight = jnp.exp(score - s_ref[block, pl.ds(2 * head, 1)])
            halves.append((weight * (grad - s_ref[block, pl.ds(2 * head + 1, 1)])).astype(jnp.bfloat16))
            weights.append(weight.astype(jnp.bfloat16))
        steps, keys, values = [], [], []
        for (block, _, picked, _, cols), weight, half in zip(items, weights, halves):
            keys.append(dot(half, q_ref[block, :, cols]) * scale)
            values.append(dot(weight, g_ref[block, :, cols]))
            steps.append((dot(half, k_ref[picked, :, cols], TN) * scale).astype(jnp.bfloat16))
        for number, (block, live, picked, _, cols) in enumerate(items):
            @pl.when(live)
            def _():
                dq_ref[block, :, cols] = steps[number]
                dk_acc[picked, :, cols] += keys[number]
                dv_acc[picked, :, cols] += values[number]

    pk_ref[...] = dk_acc[...].astype(jnp.bfloat16)
    pv_ref[...] = dv_acc[...].astype(jnp.bfloat16)


def table_of(ids):
    total = ids.shape[0]
    spot = jnp.arange(total, dtype=jnp.int32)
    idle = (ids < 0).astype(jnp.int32)
    sort_key = idle * total + spot
    rank = jnp.sum((sort_key[None, :] < sort_key[:, None]).astype(jnp.int32), axis=1)
    order = jnp.sum(jnp.where(rank[None, :] == spot[:, None], spot[None, :], 0), axis=1)
    count = total - jnp.sum(idle)
    return jnp.concatenate([ids, order, count[None]])


def query_plan(queries, gate_pre, cotangent, store, store_gain, w_key, w_value, owners, slots):
    n = lax.axis_size("st")
    tp_size = lax.axis_size("tp")
    me = lax.axis_index("st")
    blocks, per_block = owners.shape
    tok_rows, local_width = queries.shape
    heads = local_width // HD
    block_len = tok_rows // blocks
    rows_dev = store.shape[0]
    passages = rows_dev // PLEN
    named = jnp.pad(owners * passages + slots, ((0, 0), (0, 128 - per_block)), constant_values=-1)
    gate_open = jax.nn.sigmoid(gate_pre.astype(jnp.float32))
    grad_in = (gate_open * cotangent.astype(jnp.float32)).astype(jnp.bfloat16)
    q_all, g_all, all_named = ring_gather(queries, grad_in, named, n)
    held = all_named.reshape(n * blocks, 128)[:, :per_block] - me * passages
    ids = jnp.max(jnp.where((held >= 0) & (held < passages), held, -1), axis=1)
    store_rows = store.astype(jnp.float32)
    row_inverse = row_scale(store_rows)
    normed = (store_rows * row_inverse * store_gain).astype(jnp.bfloat16)
    key_table = jnp.dot(normed, w_key, preferred_element_type=jnp.float32).astype(jnp.bfloat16)
    value_table = jnp.dot(normed, w_value, preferred_element_type=jnp.float32).astype(jnp.bfloat16)
    key_table = key_table.reshape(passages, PLEN, local_width)
    value_table = value_table.reshape(passages, PLEN, local_width)
    table = table_of(ids)
    total = n * blocks
    q_blocks = q_all.reshape(total, block_len, local_width)
    g_blocks = g_all.reshape(total, block_len, local_width)
    smem = pl.BlockSpec(memory_space=pltpu.SMEM)
    vmem = pl.BlockSpec(memory_space=pltpu.VMEM)
    stats = pl.pallas_call(
        functools.partial(stats_kernel, heads),
        out_shape=jax.ShapeDtypeStruct((total, 2 * heads, block_len), jnp.float32),
        in_specs=[smem] + [vmem] * 4,
        out_specs=vmem,
        compiler_params=pltpu.CompilerParams(vmem_limit_bytes=40 << 20),
        name="stats",
    )(table, q_blocks, g_blocks, key_table, value_table)
    joined = join_stats(stats, n)
    dq, passage_keys, passage_values = pl.pallas_call(
        functools.partial(grads_kernel, heads),
        out_shape=(
            jax.ShapeDtypeStruct((total, block_len, local_width), jnp.bfloat16),
            jax.ShapeDtypeStruct((passages, PLEN, local_width), jnp.bfloat16),
            jax.ShapeDtypeStruct((passages, PLEN, local_width), jnp.bfloat16),
        ),
        in_specs=[smem] + [vmem] * 5,
        out_specs=(vmem,) * 3,
        scratch_shapes=[pltpu.VMEM((passages, PLEN, local_width), jnp.float32)] * 2,
        compiler_params=pltpu.CompilerParams(vmem_limit_bytes=40 << 20),
        name="grads",
    )(table, q_blocks, g_blocks, key_table, value_table, joined)
    dq = dq.reshape(n, tok_rows, local_width)
    passage_keys = passage_keys.reshape(rows_dev, local_width)
    passage_values = passage_values.reshape(rows_dev, local_width)
    weight_terms = lax.dot_general(
        normed, passage_values, (((0,), (0,)), ((), ())), preferred_element_type=jnp.float32
    ).astype(jnp.bfloat16)
    whole_key, whole_value = (
        lax.all_gather(w_key, "tp", axis=1, tiled=True),
        lax.all_gather(w_value, "tp", axis=1, tiled=True),
    )
    quarter = rows_dev // tp_size
    grad_queries, grad_w_value, own_keys, own_values = ring_scatter(
        dq, weight_terms.reshape(n, -1, local_width), passage_keys, passage_values, n, tp_size
    )
    grad_normed = contract(own_keys, whole_key) + contract(own_values, whole_value)
    first_row = lax.axis_index("tp") * quarter
    own_rows = lax.dynamic_slice_in_dim(store, first_row, quarter, 0).astype(jnp.float32)
    own_inverse = row_scale(own_rows)
    unit_rows = own_rows * own_inverse
    grad_unit = grad_normed * store_gain
    grad_store = own_inverse * (
        grad_unit - unit_rows * jnp.mean(grad_unit * unit_rows, axis=-1, keepdims=True)
    )
    return (grad_queries, grad_store, grad_w_value)


def local(*arrays):
    queries, owners = arrays[0], arrays[7]
    n = lax.axis_size("st")
    slot_cap = (2 * owners.size + n - 1) // n
    if n % 2 == 0 and n >= 4 and 8 * slot_cap * PLEN >= 3 * queries.shape[0]:
        return query_plan(*arrays)
    return passage_plan(*arrays)


def solution(mesh):
    placed = (
        P("st", "tp"),
        P("st", "tp"),
        P("st", "tp"),
        P("st", None),
        P(),
        P(None, "tp"),
        P(None, "tp"),
        P("st", None),
        P("st", None),
    )
    return jax.shard_map(
        local,
        mesh=mesh,
        in_specs=placed,
        out_specs=(P("st", "tp"), P(("st", "tp"), None), P("st", "tp")),
        check_vma=False,
    )
```

profile of v0, /device:TPU:0, one launch (start us, length us, event | category | flops | bytes accessed | tf_op | source)
XLA Modules:
  0.0 252.2 jit_solution(16181963017452374197)
XLA Ops:
  7.2 0.0 all-gather.3.cloned.1.call-start
  7.2 0.7 all-gather.3.cloned.1.call-update
  7.9 0.0 all-gather.5.cloned.1.call-start
  7.9 0.7 all-gather.5.cloned.1.call-update
  8.7 0.8 copy.14
  9.4 0.8 copy.15
  10.2 1.5 multiply_convert_fusion.g_ref
  11.7 0.0 copy-start.8
  11.7 1.0 copy-done.8
  12.7 84.9 %ring_gather.1 = (bf16[8,1024,256]{2,1,0:T(8,128)(2,1)S(1)}, bf16[8,1024,256]{2,1,0:T(8,128)(2,1)S(1)}, s32[8,8,128]{2,1,0:T(8,128)S(1)}) custom-call(bf16[1024,256]{1,0:T(8,128)(2,1)S(1)} %copy-done.8, bf16[1024,256]{1,0:T(8,128)(2,1)S(1)} %multiply_convert_fusion.g_ref, s32[8,128]{1,0:T(8,128)S(1)} %pad.4.i_ref), custom_call_target="tpu_custom_call" | custom-call | flops 10000000000 | bytes 10000000 | tf_op jit(solution)/shard_map/ring_gather/pallas_call | solution.py:240
  97.6 0.0 copy-start
  97.6 1.9 copy-done
  99.5 2.0 copy-done.3
  101.5 0.1 select_reduce_fusion.1
  101.6 0.6 fusion.10
  102.9 0.2 convert_reduce_fusion
  103.1 0.1 select_reduce_fusion
  103.2 0.1 pad_add_fusion.table
  103.3 3.7 %fusion = f32[1280]{0:T(1024)S(1)} fusion(bf16[1280,2048]{1,0:T(8,128)(2,1)} %param.12), kind=kLoop, calls=%fused_computation.2 | loop fusion | flops 7863040 | bytes 5248000 | tf_op jit(solution)/shard_map/reduce_sum | solution.py:18
  107.0 0.0 copy-done.10
  107.1 0.0 copy-done.12
  107.1 0.0 slice-start.1
  107.1 0.0 copy-start.11
  107.1 4.3 %convolution_convert_fusion.2 = bf16[1280,256]{1,0:T(8,128)(2,1)S(1)} fusion(bf16[2048,256]{1,0:T(8,128)(2,1)S(1)} %copy-done.10, bf16[1280,2048]{1,0:T(8,128)(2,1)} %param.12, f32[2048]{0:T(1024)S(1)} %copy-done.12, f32[1280]{0:T(1024)S(1)} %add_rsqrt_fusion), kind=kOutput, calls=%fused_computation.17 | convolution fusion | flops 1352990720 | bytes 6960128 | tf_op jit(solution)/shard_map/dot_general | solution.py:545
  111.3 0.0 slice-done
  111.4 1.6 convolution_convert_fusion.1
  113.0 0.5 copy-done.1
  113.6 1.3 copy-done.4
  114.9 3.6 %stats.1 = f32[64,4,128]{2,1,0:T(4,128)S(1)} custom-call(s32[129]{0:T(256)S(1)} %pad_add_fusion.table, bf16[64,128,256]{2,1,0:T(8,128)(2,1)S(1)} %bitcast.19, bf16[64,128,256]{2,1,0:T(8,128)(2,1)S(1)} %bitcast.22, bf16[20,64,256]{2,1,0:T(8,128)(2,1)S(1)} %bitcast.23, bf16[20,64,256]{2,1,0:T(8,128)(2,1)S(1)} %bitcast.25), custom_call_target="tpu_custom_call" | custom-call | tf_op jit(solution)/shard_map/stats/pallas_call | solution.py:555
  118.4 0.0 copy-start.6
  118.5 0.6 copy-done.6
  119.1 20.5 %join_stats.1 = f32[8,8,4,128]{3,2,1,0:T(4,128)} custom-call(f32[8,8,4,128]{3,2,1,0:T(4,128)} %bitcast.28), custom_call_target="tpu_custom_call" | custom-call | flops 1000000000 | bytes 1000000 | tf_op jit(solution)/shard_map/join_stats/pallas_call | solution.py:297
  139.6 0.0 copy-start.2
  139.6 2.2 copy-done.2
  141.8 0.9 copy-done.5
  142.7 8.2 %grads.1 = (bf16[64,128,256]{2,1,0:T(8,128)(2,1)S(1)}, bf16[20,64,256]{2,1,0:T(8,128)(2,1)S(1)}, bf16[20,64,256]{2,1,0:T(8,128)(2,1)S(1)}) custom-call(s32[129]{0:T(256)S(1)} %pad_add_fusion.table, bf16[64,128,256]{2,1,0:T(8,128)(2,1)S(1)} %bitcast.20, bf16[64,128,256]{2,1,0:T(8,128)(2,1)} %bitcast.21, bf16[20,64,256]{2,1,0:T(8,128)(2,1)S(1)} %bitcast.24, ...), custom_call_target="tpu_custom_call" | custom-call | tf_op jit(solution)/shard_map/grads/pallas_call | solution.py:564
  150.9 2.0 copy-done.7
  152.8 5.5 %convolution_convert_fusion = bf16[2048,256]{1,0:T(8,128)(2,1)} fusion(bf16[1280,256]{1,0:T(8,128)(2,1)S(1)} %bitcast.32, bf16[1280,2048]{1,0:T(8,128)(2,1)} %param.12, f32[2048]{0:T(1024)S(1)} %copy-done.12, f32[1280]{0:T(1024)S(1)} %add_rsqrt_fusion), kind=kOutput, calls=%fused_computation.15 | convolution fusion | flops 1353187328 | bytes 6960128 | tf_op jit(solution)/shard_map/dot_general | solution.py:580
  158.4 68.7 %ring_scatter.1 = (f32[1024,256]{1,0:T(8,128)S(1)}, f32[256,256]{1,0:T(8,128)S(1)}, bf16[320,1024]{1,0:T(8,128)(2,1)S(1)}, bf16[320,1024]{1,0:T(8,128)(2,1)S(1)}) custom-call(bf16[8,1024,256]{2,1,0:T(8,128)(2,1)} %bitcast.30, bf16[8,256,256]{2,1,0:T(8,128)(2,1)} %bitcast.36, bf16[1280,256]{1,0:T(8,128)(2,1)S(1)} %bitcast.31, bf16[1280,256]{1,0:T(8,128)(2,1)S(1)} %bitcast.33), custom_call_target="tpu_custom_call" | custom-call | flops 5000000000 | bytes 10000000 | tf_op jit(solution)/shard_map/ring_scatter/pallas_call | solution.py:405
  227.1 0.0 copy-start.9
  227.1 0.8 copy-done.9
  227.9 1.7 fusion.9
  229.6 0.0 all-gather.3.cloned.1.call-done
  229.6 5.4 %fusion.15 = f32[320,2048]{1,0:T(8,128)} fusion(bf16[320,1024]{1,0:T(8,128)(2,1)} %copy-done.9, bf16[2048,1024]{1,0:T(8,128)(2,1)} %all-gather.3.cloned.1.call-done), kind=kOutput, calls=%fused_computation.33 | convolution fusion | flops 1342177280 | bytes 7471104 | tf_op jit(solution)/shard_map/dot_general | solution.py:22
  235.1 5.2 %fusion.6 = (f32[320]{0:T(512)S(1)}, f32[320,2048]{1,0:T(8,128)S(1)}) fusion(f32[320]{0:T(512)S(1)} %add_rsqrt_fusion.1, bf16[1280,2048]{1,0:T(8,128)(2,1)} %param.12, s32[]{:T(128)S(6)} %select_n.13, f32[2048]{0:T(1024)S(1)} %copy-done.12, f32[320,2048]{1,0:T(8,128)} %fusion.15, bf16[320,1024]{1,0:T(8,128)(2,1)S(1)} %get-tuple-element.21, ...), kind=kOutput, calls=%fused_computation.11 | convolution fusion | flops 1346109184 | bytes 11414020 | tf_op jit(solution)/shard_map/dot_general | solution.py:22
  240.3 3.3 %fusion.8 = f32[320,2048]{1,0:T(8,128)} fusion(f32[320,2048]{1,0:T(8,128)S(1)} %get-tuple-element.26, f32[320]{0:T(512)S(1)} %broadcast_multiply_fusion, f32[320]{0:T(512)S(1)} %add_rsqrt_fusion.1, bf16[1280,2048]{1,0:T(8,128)(2,1)} %param.12, s32[]{:T(128)S(6)} %select_n.13), kind=kLoop, calls=%fused_computation.13 | loop fusion | flops 3276800 | bytes 6556164 | tf_op jit(solution)/shard_map/mul | solution.py:597
  243.6 1.0 copy.18
  244.6 0.7 copy.19
  (17 shorter events, 0.1 us)
Async XLA Ops:
  7.2 222.4 %all-gather.3.cloned.1.call-start = ((), (), s32[]{:S(2)}) async-start(), calls=%async_computation | async-start | bytes 5242880 | tf_op jit(solution)/shard_map/all_gather | solution.py:584
  7.9 227.2 %all-gather.5.cloned.1.call-start = ((), (), s32[]{:S(2)}) async-start(), calls=%async_computation.1 | async-start | bytes 5242880 | tf_op jit(solution)/shard_map/all_gather | solution.py:585
  11.7 1.0 copy-start.8
  97.6 1.9 copy-start
  99.5 2.0 copy-start.3
  101.5 5.5 %copy-start.10 = (bf16[2048,256]{1,0:T(8,128)(2,1)S(1)}, bf16[2048,256]{1,0:T(8,128)(2,1)}, u32[]{:S(2)}) copy-start(bf16[2048,256]{1,0:T(8,128)(2,1)} %param.14) | copy-start | bytes 3145732
  101.5 5.5 %copy-start.12 = (f32[2048]{0:T(1024)S(1)}, f32[2048]{0:T(1024)}, u32[]{:S(2)}) copy-start(f32[2048]{0:T(1024)} %param.13) | copy-start | bytes 24580
  103.3 8.1 %slice-start = ((s8[5242880]{0:T(1024)(128)(4,1)}), s8[4194304]{0:T(1024)(128)(4,1)S(1)}, s32[]{:S(2)}) async-start(s8[5242880]{0:T(1024)(128)(4,1)} %bitcast.34), calls=%async_computation.2 | async-start | bytes 8388608
  107.1 4.3 %slice-start.1 = ((s8[5242880]{0:T(1024)(128)(4,1)}), s8[1048576]{0:T(1024)(128)(4,1)S(1)}, s32[]{:S(2)}) async-start(s8[5242880]{0:T(1024)(128)(4,1)} %bitcast.34), calls=%async_computation.3 | async-start | bytes 2097152
  107.1 4.3 %copy-start.11 = (bf16[2048,256]{1,0:T(8,128)(2,1)S(1)}, bf16[2048,256]{1,0:T(8,128)(2,1)}, u32[]{:S(2)}) copy-start(bf16[2048,256]{1,0:T(8,128)(2,1)} %param.15) | copy-start | bytes 3145732
  111.4 2.2 copy-start.1
  111.4 3.5 %copy-start.4 = (bf16[8,1024,256]{2,1,0:T(8,128)(2,1)S(1)}, bf16[8,1024,256]{2,1,0:T(8,128)(2,1)}, u32[]{:S(2)}) copy-start(bf16[8,1024,256]{2,1,0:T(8,128)(2,1)} %copy-done.3) | copy-start | bytes 12582916
  118.4 0.7 copy-start.6
  139.6 2.2 copy-start.2
  141.8 0.9 copy-start.5
  150.9 2.0 copy-start.7
  227.1 0.8 copy-start.9
Sparse Core Ops, SparseCore 0:
  9.5 37.7 all-gather.2
  48.8 34.9 all-gather.4
where the time goes:
time: 250 us; the launch traced here: 252 us
  Pallas kernels  186 us (74%)
  matrix products  22.1 us (9%)
  local copies, waits for them, and re-layouts  16.5 us (7%)
  between operations  14.9 us (6%)
  other arithmetic  11.4 us (5%)
    pallas_call x1, Pallas kernels, ring_gather(): pl.pallas_call(functools.partial(gather_kernel, n), out_shape=tuple((jax....  84.9 us
    pallas_call x1, Pallas kernels, ring_scatter(): pl.pallas_call(functools.partial(scatter_kernel, n, tp, parts), out_shape...  68.7 us
    pallas_call x1, Pallas kernels, join_stats(): pl.pallas_call(functools.partial(join_kernel, n, rows // 2), out_shape=ja...  20.5 us
    unnamed x34, local copies, waits for them, and re-layouts  16.5 us
    dot_general x2, matrix products, contract(): lax.dot_general(left, right, (((1,), (1,)), ((), ())), preferred_element_...  10.7 us
    pallas_call x1, Pallas kernels, query_plan(): pl.pallas_call(functools.partial(grads_kernel, heads), out_shape=(jax.Sha...  8.22 us
    dot_general x1, matrix products, query_plan(): lax.dot_general(normed, passage_values, (((0,), (0,)), ((), ())), preferr...  5.53 us
    reduce_sum x2, other arithmetic, row_scale(): jnp.mean(store_rows * store_rows, axis=-1, keepdims=True) + EPS  5.4 us
  transfers between devices with their start and end apart: 2, of which 0 were waited for; matrix products, arithmetic and copies ran while one was open for 10% of the time, Pallas kernels for 74%

commit v1 on v0

--- a/solution.py
+++ b/solution.py
@@ -179,7 +179,7 @@
     pl.semaphore_wait(barrier, len(others))
 
 
-def gather_kernel(n, q_ref, g_ref, i_ref, q_all, g_all, i_all, send_sem, recv_sem, own_sem):
+def gather_kernel(n, q_ref, g_ref, i_ref, x_ref, gain_ref, wk_ref, wv_ref, q_all, g_all, i_all, normed_ref, kt_ref, vt_ref, send_sem, recv_sem, own_sem):
     me = lax.axis_index("st")
     place = place_of(me, n)
     right, left = index_at(place + 1, n), index_at(place - 1, n)
@@ -211,6 +211,17 @@
             device_id_type=MESH,
         )
 
+    count = x_ref.shape[0] // 128
+
+    def project(chunk):
+        rows = pl.ds(chunk * 128, 128)
+        wide = x_ref[rows].astype(jnp.float32)
+        normed = (wide * row_scale(wide) * gain_ref[...]).astype(jnp.bfloat16)
+        normed_ref[rows] = normed
+        kt_ref[rows] = jnp.dot(normed, wk_ref[...], preferred_element_type=jnp.float32).astype(jnp.bfloat16)
+        vt_ref[rows] = jnp.dot(normed, wv_ref[...], preferred_element_type=jnp.float32).astype(jnp.bfloat16)
+
+    chunk = 0
     started = []
     for step in range(hops):
         for part in range(5):
@@ -221,6 +232,11 @@
                     copy = piece(side, step, part)
                     copy.start()
                     started.append(copy)
+            if part > 0 and chunk < count:
+                project(chunk)
+                chunk += 1
+    for rest in range(chunk, count):
+        project(rest)
     for part in range(5):
         for side in range(2):
             if not last_on(side, part):
@@ -233,15 +249,17 @@
         copy.wait_send()
 
 
-def ring_gather(queries, grad_in, named, n):
+def ring_gather(queries, grad_in, named, store, gain, w_key, w_value, n):
     hops = n // 2
     vmem = pl.BlockSpec(memory_space=pltpu.VMEM)
     sources = (queries, grad_in, named)
     return pl.pallas_call(
         functools.partial(gather_kernel, n),
-        out_shape=tuple(jax.ShapeDtypeStruct((n,) + x.shape, x.dtype) for x in sources),
-        in_specs=[vmem] * 3,
-        out_specs=(vmem,) * 3,
+        out_shape=tuple(jax.ShapeDtypeStruct((n,) + x.shape, x.dtype) for x in sources)
+        + (jax.ShapeDtypeStruct(store.shape, jnp.bfloat16),)
+        + (jax.ShapeDtypeStruct((store.shape[0], w_key.shape[1]), jnp.bfloat16),) * 2,
+        in_specs=[vmem] * 7,
+        out_specs=(vmem,) * 6,
         scratch_shapes=[
             pltpu.SemaphoreType.DMA((2, hops, 5)),
             pltpu.SemaphoreType.DMA((2, hops, 5)),
@@ -250,7 +268,7 @@
         cost_estimate=pl.CostEstimate(flops=10**10, bytes_accessed=10**7, transcendentals=0),
         compiler_params=pltpu.CompilerParams(collective_id=0, has_side_effects=True, vmem_limit_bytes=40 << 20),
         name="ring_gather",
-    )(*sources)
+    )(*sources, store, gain[None], w_key, w_value)
 
 
 def join_kernel(n, heads, x_ref, out_ref, got, mine, send_sem, recv_sem, own_sem):
@@ -536,14 +554,11 @@
     named = jnp.pad(owners * passages + slots, ((0, 0), (0, 128 - per_block)), constant_values=-1)
     gate_open = jax.nn.sigmoid(gate_pre.astype(jnp.float32))
     grad_in = (gate_open * cotangent.astype(jnp.float32)).astype(jnp.bfloat16)
-    q_all, g_all, all_named = ring_gather(queries, grad_in, named, n)
+    q_all, g_all, all_named, normed, key_table, value_table = ring_gather(
+        queries, grad_in, named, store, store_gain, w_key, w_value, n
+    )
     held = all_named.reshape(n * blocks, 128)[:, :per_block] - me * passages
     ids = jnp.max(jnp.where((held >= 0) & (held < passages), held, -1), axis=1)
-    store_rows = store.astype(jnp.float32)
-    row_inverse = row_scale(store_rows)
-    normed = (store_rows * row_inverse * store_gain).astype(jnp.bfloat16)
-    key_table = jnp.dot(normed, w_key, preferred_element_type=jnp.float32).astype(jnp.bfloat16)
-    value_table = jnp.dot(normed, w_value, preferred_element_type=jnp.float32).astype(jnp.bfloat16)
     key_table = key_table.reshape(passages, PLEN, local_width)
     value_table = value_table.reshape(passages, PLEN, local_width)
     table = table_of(ids)

time: 250 us -> 248 us (level); the launches traced: 252 us -> 244 us
  matrix products: 22.1 us -> 15.7 us
  other arithmetic: 11.4 us -> 7.64 us
  local copies, waits for them, and re-layouts: 16.5 us -> 19.1 us
    pallas_call x1, Pallas kernels: 68.7 us -> 54.7 us  [ring_scatter(): pl.pallas_call(functools.partial(scatter_kernel, n, tp, parts), out_shape...]
    pallas_call x1, Pallas kernels: 8.22 us -> 15.3 us  [query_plan(): pl.pallas_call(functools.partial(grads_kernel, heads), out_shape=(jax.Sha...]
    dot_general x2 -> x0, matrix products: 5.88 us -> none  [the longest x1 4.25 us: query_plan(): jnp.dot(normed, w_key, preferred_element_type=jnp.float32)]
    pallas_call x1, Pallas kernels: 84.9 us -> 89.7 us  [ring_gather(): pl.pallas_call(functools.partial(gather_kernel, n), out_shape=tuple((jax....]
    pallas_call x1, Pallas kernels: 3.58 us -> 7.32 us  [query_plan(): pl.pallas_call(functools.partial(stats_kernel, heads), out_shape=jax.Shap...]
    reduce_sum x2 -> x1, other arithmetic: 5.4 us -> 1.67 us  [row_scale(): jnp.mean(store_rows * store_rows, axis=-1, keepdims=True) + EPS]
    unnamed x34 -> x30, local copies, waits for them, and re-layouts: 16.5 us -> 19.1 us
    pallas_call x1, Pallas kernels: 20.5 us -> 17.9 us  [join_stats(): pl.pallas_call(functools.partial(join_kernel, n, rows // 2), out_shape=ja...]
  transfers between devices with their start and end apart: 2 -> 2, of which waited for: 0 -> 0; matrix products, arithmetic and copies ran while one was open for 10% -> 7% of each run, Pallas kernels for 74% -> 76%
where the time goes in v1:
time: 248 us; the launch traced here: 244 us
  Pallas kernels  185 us (75%)
  local copies, waits for them, and re-layouts  19.1 us (8%)
  matrix products  15.7 us (6%)
  between operations  14.9 us (6%)
  other arithmetic  7.64 us (3%)
    pallas_call x1, Pallas kernels, ring_gather(): pl.pallas_call(functools.partial(gather_kernel, n), out_shape=tuple((jax....  89.7 us
    pallas_call x1, Pallas kernels, ring_scatter(): pl.pallas_call(functools.partial(scatter_kernel, n, tp, parts), out_shape...  54.7 us
    unnamed x30, local copies, waits for them, and re-layouts  19.1 us
    pallas_call x1, Pallas kernels, join_stats(): pl.pallas_call(functools.partial(join_kernel, n, rows // 2), out_shape=ja...  17.9 us
    pallas_call x1, Pallas kernels, query_plan(): pl.pallas_call(functools.partial(grads_kernel, heads), out_shape=(jax.Sha...  15.3 us
    dot_general x2, matrix products, contract(): lax.dot_general(left, right, (((1,), (1,)), ((), ())), preferred_element_...  10.6 us
    pallas_call x1, Pallas kernels, query_plan(): pl.pallas_call(functools.partial(stats_kernel, heads), out_shape=jax.Shap...  7.32 us
    dot_general x1, matrix products, query_plan(): lax.dot_general(normed, passage_values, (((0,), (0,)), ((), ())), preferr...  5.07 us
  transfers between devices with their start and end apart: 2, of which 0 were waited for; matrix products, arithmetic and copies ran while one was open for 7% of the time, Pallas kernels for 76%

profile of v1, /device:TPU:0, one launch (start us, length us, event | category | flops | bytes accessed | tf_op | source)
XLA Modules:
  0.0 243.7 jit_solution(10757542216413291179)
XLA Ops:
  7.2 0.0 copy-start.5
  7.2 0.0 copy-start.6
  7.2 0.0 copy-start.11
  7.2 0.0 all-gather.3.cloned.1.call-start
  7.2 0.7 all-gather.3.cloned.1.call-update
  7.9 0.0 all-gather.5.cloned.1.call-start
  8.0 0.7 all-gather.5.cloned.1.call-update
  8.7 0.8 copy.14
  9.4 0.8 copy.15
  10.2 1.5 multiply_convert_fusion.g_ref
  11.7 0.0 copy-done.5
  11.7 0.0 copy-done.6
  11.7 0.0 copy-done.11
  11.8 0.0 copy-start.10
  11.8 1.0 copy-done.10
  12.8 89.7 %ring_gather.1 = (bf16[8,1024,256]{2,1,0:T(8,128)(2,1)S(1)}, bf16[8,1024,256]{2,1,0:T(8,128)(2,1)S(1)}, s32[8,8,128]{2,1,0:T(8,128)S(1)}, bf16[1280,2048]{1,0:T(...) custom-call(bf16[1024,256]{1,0:T(8,128)(2,1)S(1)} %copy-done.10, ...), custom_call_target="tpu_custom_call" | custom-call | flops 10000000000 | bytes 10000000 | tf_op jit(solution)/shard_map/ring_gather/pallas_call | solution.py:256
  102.5 0.0 copy-start
  102.5 2.0 copy-done
  104.5 0.0 copy-start.3
  104.5 1.9 copy-done.3
  106.4 0.1 select_reduce_fusion.1
  106.5 0.6 fusion.7
  107.8 0.2 convert_reduce_fusion
  108.0 0.1 select_reduce_fusion
  108.1 0.1 pad_add_fusion.table
  108.2 2.2 copy-done.1
  110.4 2.2 copy-done.4
  112.6 7.3 %stats.1 = f32[64,4,128]{2,1,0:T(4,128)S(1)} custom-call(s32[129]{0:T(256)S(1)} %pad_add_fusion.table, bf16[64,128,256]{2,1,0:T(8,128)(2,1)S(1)} %bitcast.19, bf16[64,128,256]{2,1,0:T(8,128)(2,1)S(1)} %bitcast.22, bf16[20,64,256]{2,1,0:T(8,128)(2,1)S(1)} %bitcast.23, bf16[20,64,256]{2,1,0:T(8,128)(2,1)S(1)} %bitcast.25), custom_call_target="tpu_custom_call" | custom-call | tf_op jit(solution)/shard_map/stats/pallas_call | solution.py:570
  119.9 0.0 copy-start.8
  119.9 0.6 copy-done.8
  120.6 17.9 %join_stats.1 = f32[8,8,4,128]{3,2,1,0:T(4,128)} custom-call(f32[8,8,4,128]{3,2,1,0:T(4,128)} %bitcast.28), custom_call_target="tpu_custom_call" | custom-call | flops 1000000000 | bytes 1000000 | tf_op jit(solution)/shard_map/join_stats/pallas_call | solution.py:315
  138.5 0.0 copy-start.2
  138.5 2.2 copy-done.2
  140.7 0.9 copy-done.7
  141.6 15.3 %grads.1 = (bf16[64,128,256]{2,1,0:T(8,128)(2,1)S(1)}, bf16[20,64,256]{2,1,0:T(8,128)(2,1)S(1)}, bf16[20,64,256]{2,1,0:T(8,128)(2,1)S(1)}) custom-call(s32[129]{0:T(256)S(1)} %pad_add_fusion.table, bf16[64,128,256]{2,1,0:T(8,128)(2,1)S(1)} %bitcast.20, bf16[64,128,256]{2,1,0:T(8,128)(2,1)} %bitcast.21, bf16[20,64,256]{2,1,0:T(8,128)(2,1)S(1)} %bitcast.24, ...), custom_call_target="tpu_custom_call" | custom-call | tf_op jit(solution)/shard_map/grads/pallas_call | solution.py:579
  156.9 0.0 copy-start.9
  156.9 1.9 copy-done.9
  158.8 5.1 %convolution_convert_fusion = bf16[2048,256]{1,0:T(8,128)(2,1)} fusion(bf16[1280,2048]{1,0:T(8,128)(2,1)} %get-tuple-element.22, bf16[1280,256]{1,0:T(8,128)(2,1)S(1)} %bitcast.32), kind=kOutput, calls=%fused_computation.10 | convolution fusion | flops 1342701568 | bytes 6946816 | tf_op jit(solution)/shard_map/dot_general | solution.py:595
  163.9 54.7 %ring_scatter.1 = (f32[1024,256]{1,0:T(8,128)S(1)}, f32[256,256]{1,0:T(8,128)S(1)}, bf16[320,1024]{1,0:T(8,128)(2,1)S(1)}, bf16[320,1024]{1,0:T(8,128)(2,1)S(1)}) custom-call(bf16[8,1024,256]{2,1,0:T(8,128)(2,1)} %bitcast.30, bf16[8,256,256]{2,1,0:T(8,128)(2,1)} %bitcast.35, bf16[1280,256]{1,0:T(8,128)(2,1)S(1)} %bitcast.31, bf16[1280,256]{1,0:T(8,128)(2,1)S(1)} %bitcast.33), custom_call_target="tpu_custom_call" | custom-call | flops 5000000000 | bytes 10000000 | tf_op jit(solution)/shard_map/ring_scatter/pallas_call | solution.py:423
  218.6 0.0 copy-start.12
  218.6 0.8 copy-done.12
  219.5 1.7 fusion.6
  221.1 0.0 all-gather.3.cloned.1.call-done
  221.2 5.5 %fusion.9 = f32[320,2048]{1,0:T(8,128)} fusion(bf16[320,1024]{1,0:T(8,128)(2,1)} %copy-done.12, bf16[2048,1024]{1,0:T(8,128)(2,1)} %all-gather.3.cloned.1.call-done), kind=kOutput, calls=%fused_computation.25 | convolution fusion | flops 1342177280 | bytes 7471104 | tf_op jit(solution)/shard_map/dot_general | solution.py:22
  226.6 5.2 %fusion.3 = (f32[320]{0:T(512)S(1)}, f32[320,2048]{1,0:T(8,128)S(1)}) fusion(f32[320]{0:T(512)S(1)} %add_rsqrt_fusion, bf16[1280,2048]{1,0:T(8,128)(2,1)} %x_ref.1, s32[]{:T(128)S(6)} %select_n.13, f32[2048]{0:T(1024)S(1)} %copy-done.11, f32[320,2048]{1,0:T(8,128)} %fusion.9, bf16[320,1024]{1,0:T(8,128)(2,1)S(1)} %get-tuple-element.27, ...), kind=kOutput, calls=%fused_computation.6 | convolution fusion | flops 1346109184 | bytes 11414020 | tf_op jit(solution)/shard_map/dot_general | solution.py:22
  231.8 3.3 %fusion.5 = f32[320,2048]{1,0:T(8,128)} fusion(f32[320,2048]{1,0:T(8,128)S(1)} %get-tuple-element.32, f32[320]{0:T(512)S(1)} %broadcast_multiply_fusion, f32[320]{0:T(512)S(1)} %add_rsqrt_fusion, bf16[1280,2048]{1,0:T(8,128)(2,1)} %x_ref.1, s32[]{:T(128)S(6)} %select_n.13), kind=kLoop, calls=%fused_computation.8 | loop fusion | flops 3276800 | bytes 6556164 | tf_op jit(solution)/shard_map/mul | solution.py:612
  235.2 1.0 copy.18
  236.1 0.7 copy.19
  (8 shorter events, 0.0 us)
Async XLA Ops:
  7.2 4.6 %copy-start.5 = (bf16[2048,256]{1,0:T(8,128)(2,1)S(1)}, bf16[2048,256]{1,0:T(8,128)(2,1)}, u32[]{:S(2)}) copy-start(bf16[2048,256]{1,0:T(8,128)(2,1)} %wk_ref.1) | copy-start | bytes 3145732
  7.2 4.6 %copy-start.6 = (bf16[2048,256]{1,0:T(8,128)(2,1)S(1)}, bf16[2048,256]{1,0:T(8,128)(2,1)}, u32[]{:S(2)}) copy-start(bf16[2048,256]{1,0:T(8,128)(2,1)} %wv_ref.1) | copy-start | bytes 3145732
  7.2 4.6 %copy-start.11 = (f32[2048]{0:T(1024)S(1)}, f32[2048]{0:T(1024)}, u32[]{:S(2)}) copy-start(f32[2048]{0:T(1024)} %param.13) | copy-start | bytes 24580
  7.2 214.0 %all-gather.3.cloned.1.call-start = ((), (), s32[]{:S(2)}) async-start(), calls=%async_computation | async-start | bytes 5242880 | tf_op jit(solution)/shard_map/all_gather | solution.py:599
  7.9 218.7 %all-gather.5.cloned.1.call-start = ((), (), s32[]{:S(2)}) async-start(), calls=%async_computation.1 | async-start | bytes 5242880 | tf_op jit(solution)/shard_map/all_gather | solution.py:600
  11.8 1.0 copy-start.10
  102.5 2.0 copy-start
  104.5 1.9 copy-start.3
  108.2 2.2 copy-start.1
  110.4 2.2 copy-start.4
  119.9 0.7 copy-start.8
  138.5 2.2 copy-start.2
  140.7 0.9 copy-start.7
  156.9 1.9 copy-start.9
  218.6 0.8 copy-start.12
Sparse Core Ops, SparseCore 0:
  9.6 37.7 all-gather.2
  48.9 34.9 all-gather.4
